TPU v7x, 32 devices: a whole 2x2x4 slice. The times are simulated.
32 devices in a mesh: kv: 8 (over z, y), tp: 4 (over x, core).
Axes of the slice: x: 2, y: 2, z: 4, core: 2. Of those that a mesh axis runs over, the one named last changes fastest.
Arguments:
- tokens: bfloat16 [64, 4096], P(None, 'kv'), may hold values from -170 to 170
- mix_gain: float32 [4096], P('kv'), may hold values from 0.1 to 1.9
- w_query: bfloat16 [4096, 2048], P('kv', 'tp'), may hold values from -0.09375 to 0.09375
- w_key: bfloat16 [4096, 512], P('kv', 'tp'), may hold values from -0.09375 to 0.09375
- w_value: bfloat16 [4096, 512], P('kv', 'tp'), may hold values from -0.09375 to 0.09375
- w_forget: bfloat16 [4096, 32], P('kv', 'tp'), may hold values from -0.09375 to 0.09375
- query_gain: float32 [64], replicated, may hold values from 0.1 to 1.9
- key_cache: bfloat16 [64, 8, 64, 8192], P(None, 'tp', None, 'kv'), may hold values from -1300 to 1300
- value_cache: bfloat16 [64, 8, 64, 8192], P(None, 'tp', None, 'kv'), may hold values from -8 to 8
- decay_cache: float32 [64, 32, 8192], P(None, 'tp', 'kv'), may hold values from -1066.96 to 0, as said below
- w_out: bfloat16 [2048, 4096], P('tp', 'kv'), may hold values from -1 to 1
- mlp_gain: float32 [4096], P('kv'), may hold values from 0.1 to 1.9
- w_up: bfloat16 [4096, 16384], P('kv', 'tp'), may hold values from -0.09375 to 0.09375
- w_down: bfloat16 [16384, 4096], P('tp', 'kv'), may hold values from -0.046875 to 0.046875
Outputs:
- layer_out: bfloat16 [64, 4096], P(None, 'kv')
Inputs may be any that keep to these rules, and one draw needn't show every extreme that they name: `decay_cache`: each entry is the sum of the non-positive log forget gates of the later cached positions of its sequence and head: 0 at the last cached position, never smaller at a later position.
All inputs are finite; a program needn't handle non-finite values.
Results may differ from a plain program's by a relative error of at most 0.015.
Values may be sent and summed in bfloat16 or wider, within the bound.
A program may use at most 128 MiB of HBM per device.

v0:
```python
import jax
import jax.numpy as jnp
from jax import lax
from jax.sharding import PartitionSpec as P

D = 4096
HEAD_DIM = 64


EPS = 1e-06


def shards(
    tokens,
    mix_gain,
    w_query,
    w_key,
    w_value,
    w_forget,
    query_gain,
    key_cache,
    value_cache,
    decay_cache,
    w_out,
    mlp_gain,
    w_up,
    w_down,
):
    row_count = tokens.shape[0]
    local_heads = w_forget.shape[1]
    local_groups = key_cache.shape[1]
    sharing = local_heads // local_groups
    score_scale = HEAD_DIM ** (-0.5)
    stream = tokens.astype(jnp.float32)
    squares_mix = jnp.sum(stream * stream, axis=1)
    normed_mix = (stream * mix_gain).astype(jnp.bfloat16)
    query_terms = jnp.dot(normed_mix, w_query, preferred_element_type=jnp.float32)
    key_terms = jnp.dot(normed_mix, w_key, preferred_element_type=jnp.float32)
    value_terms = jnp.dot(normed_mix, w_value, preferred_element_type=jnp.float32)
    forget_terms = jnp.dot(normed_mix, w_forget, preferred_element_type=jnp.float32)
    query_raw, key_raw, value_raw, forget_raw, total_mix = lax.psum(
        (query_terms, key_terms, value_terms, forget_terms, squares_mix), "kv"
    )
    scale_mix = lax.rsqrt(total_mix / D + EPS)[:, None]
    heads_raw = (scale_mix * query_raw).reshape(row_count, local_heads, HEAD_DIM)
    inverse = lax.rsqrt(jnp.mean(heads_raw * heads_raw, axis=-1, keepdims=True) + EPS)
    query = (heads_raw * inverse * query_gain).astype(jnp.bfloat16)
    query = query.reshape(row_count, local_groups, sharing, HEAD_DIM)
    key_new = (scale_mix * key_raw).reshape(row_count, local_groups, HEAD_DIM).astype(jnp.bfloat16)
    value_new = (
        (scale_mix * value_raw).reshape(row_count, local_groups, HEAD_DIM).astype(jnp.bfloat16)
    )
    log_forget = jax.nn.log_sigmoid(scale_mix * forget_raw).reshape(
        row_count, local_groups, sharing
    )
    decay = decay_cache.reshape(row_count, local_groups, sharing, -1)
    scores = (
        jnp.einsum("bgjd,bgdp->bgjp", query, key_cache, preferred_element_type=jnp.float32)
        * score_scale
    )
    scores = scores + decay + log_forget[..., None]
    own_score = (
        jnp.einsum("bgjd,bgd->bgj", query, key_new, preferred_element_type=jnp.float32)
        * score_scale
    )
    local_peak = jnp.max(scores, axis=-1)
    peak_score = jnp.maximum(lax.pmax(local_peak, "kv"), own_score)
    weights = jnp.exp(scores - peak_score[..., None])
    partial_values = jnp.einsum(
        "bgjp,bgdp->bgjd",
        weights.astype(jnp.bfloat16),
        value_cache,
        preferred_element_type=jnp.float32,
    )
    mass_sum, summed = lax.psum((jnp.sum(weights, axis=-1), partial_values), "kv")
    own_weight = jnp.exp(own_score - peak_score)
    totals = mass_sum + own_weight
    own_rounded = lax.optimization_barrier(own_weight.astype(jnp.bfloat16)).astype(jnp.float32)
    summed = summed + own_rounded[..., None] * value_new.astype(jnp.float32)[:, :, None, :]
    head_output = summed / totals[..., None]
    attended = head_output.reshape(row_count, local_heads * HEAD_DIM).astype(jnp.bfloat16)
    attn_terms = jnp.dot(attended, w_out, preferred_element_type=jnp.float32)
    attn_out = lax.psum(attn_terms.astype(jnp.bfloat16), "tp")
    attn_rounded = lax.optimization_barrier(attn_out).astype(jnp.float32)
    residual = (stream + attn_rounded).astype(jnp.bfloat16)
    residual_wide = residual.astype(jnp.float32)
    squares_mlp = jnp.sum(residual_wide * residual_wide, axis=1)
    normed_mlp = (residual_wide * mlp_gain).astype(jnp.bfloat16)
    up_terms = jnp.dot(normed_mlp, w_up, preferred_element_type=jnp.float32)
    up_full, total_mlp = lax.psum((up_terms, squares_mlp), "kv")
    scale_mlp = lax.rsqrt(total_mlp / D + EPS)[:, None]
    hidden = jnp.square(jax.nn.relu(scale_mlp * up_full)).astype(jnp.bfloat16)
    down_terms = jnp.dot(hidden, w_down, preferred_element_type=jnp.float32)
    mlp_out = lax.psum(down_terms.astype(jnp.bfloat16), "tp")
    mlp_rounded = lax.optimization_barrier(mlp_out).astype(jnp.float32)
    return (residual_wide + mlp_rounded).astype(jnp.bfloat16)


def solution(mesh):
    in_specs = (
        P(None, "kv"),
        P("kv"),
        P("kv", "tp"),
        P("kv", "tp"),
        P("kv", "tp"),
        P("kv", "tp"),
        P(),
        P(None, "tp", None, "kv"),
        P(None, "tp", None, "kv"),
        P(None, "tp", "kv"),
        P("tp", "kv"),
        P("kv"),
        P("kv", "tp"),
        P("tp", "kv"),
    )
    out_specs = P(None, "kv")
    return jax.shard_map(shards, mesh=mesh, in_specs=in_specs, out_specs=out_specs, check_vma=False)
```

profile of v0, /device:TPU:0, one launch (start us, length us, event | category | flops | bytes accessed | tf_op | source)
XLA Modules:
  0.0 406.1 jit_solution(14472312958995943851)
XLA Ops:
  6.5 1.0 copy-done
  7.6 1.7 fusion.23
  9.3 0.0 all-reduce.8.cloned.1.call-update
  9.3 0.0 all-reduce.10.cloned.1.call-start
  9.4 1.0 fusion.8
  10.3 1.1 fusion.19
  11.4 1.0 fusion.21
  12.4 39.3 %all-reduce.1 = (f32[64]{0:T(128)S(1)}, f32[64,8]{0,1:T(8,128)S(1)}, f32[64,128]{1,0:T(8,128)S(1)}) all-reduce(f32[64]{0:T(128)S(1)} %fusion.8, f32[64,8]{0,1:T(8,128)S(1)} %fusion.21, f32[64,128]{1,0:T(8,128)S(1)} %fusion.19), channel_id=1, replica_groups=mesh['kv'=8,'tp'=4] {'kv'}, use_global_device_ids=true, to_apply=%region_1.0 | all-reduce | flops 8768 | bytes 70144 | tf_op jit(solution)/shard_map/psum | solution.py:41
  51.7 0.1 copy.23
  51.9 2.0 reshape.49
  53.9 0.1 multiply_convert_fusion.4
  54.0 0.1 reshape.54
  54.1 0.2 fusion.17
  54.2 29.6 %all-reduce.8.cloned.1.call-done = f32[64,512]{1,0:T(8,128)} async-done(((f32[64,512]{1,0:T(8,128)}), f32[64,512]{1,0:T(8,128)}) %all-reduce.8.cloned.1.call-update) | async-done | bytes 131088 | tf_op jit(solution)/shard_map/psum | solution.py:41
  83.8 1.0 fusion.31
  84.8 0.1 mul.115
  84.9 0.1 reduce_sum.37
  85.1 0.1 copy.21
  85.1 0.1 copy.22
  85.3 0.2 reshape.48
  85.5 0.2 multiply_convert_fusion.2
  85.7 9.4 %fusion.32 = (f32[64,2,4]{2,1,0:T(2,128)S(1)}, f32[64,2,4,1024]{3,2,1,0:T(4,128)}) fusion(f32[64,2,4]{2,1,0:T(2,128)S(1)} %copy.23, f32[64,2,4,1024]{3,2,1,0:T(4,128)S(1)} %reshape.49, bf16[64,2,4,64]{3,2,1,0:T(4,128)(2,1)S(1)} %multiply_convert_fusion.2, bf16[64,2,64,1024]{3,2,1,0:T(8,128)(2,1)} %param.21), kind=kOutput, calls=%fused_computation.47 | convolution fusion | flops 69205504 | bytes 21041152 | tf_op jit(solution)/shard_map/bgjd,bgdp->bgjp/dot_general | solution.py:58
  95.1 35.9 %pmax.7 = f32[64,2,4]{2,1,0:T(2,128)S(1)} all-reduce(f32[64,2,4]{2,1,0:T(2,128)S(1)} %get-tuple-element.14), channel_id=1, replica_groups=mesh['kv'=8,'tp'=4] {'kv'}, use_global_device_ids=true, to_apply=%region_6.0 | all-reduce | flops 512 | bytes 4096 | tf_op jit(solution)/shard_map/pmax | solution.py:67
  131.0 0.3 fusion.33
  131.3 2.6 fusion
  133.9 33.9 %all-reduce = (f32[64,2,4]{2,1,0:T(2,128)S(1)}, f32[64,128]{1,0:T(8,128)S(1)}) all-reduce(f32[64,2,4]{2,1,0:T(2,128)S(1)} %fusion, f32[64,128]{1,0:T(8,128)S(1)} %fusion.17), channel_id=1, replica_groups=mesh['kv'=8,'tp'=4] {'kv'}, use_global_device_ids=true, to_apply=%region_11.12 | all-reduce | flops 8704 | bytes 69632 | tf_op jit(solution)/shard_map/psum | solution.py:75
  167.8 0.1 fusion.29
  168.0 9.0 %fusion.2 = f32[64,2,4,64]{3,2,1,0:T(4,128)} fusion(bf16[64,2,64,1024]{3,2,1,0:T(8,128)(2,1)} %param.22, f32[64,2,4,1024]{3,2,1,0:T(4,128)S(1)} %copy-done.1, f32[64,2,4]{2,1,0:T(2,128)S(1)} %multiply_maximum_fusion), kind=kOutput, calls=%fused_computation.6 | convolution fusion | flops 68157440 | bytes 19007488 | tf_op jit(solution)/shard_map/bgjp,bgdp->bgjd/dot_general | solution.py:69
  176.9 0.0 all-reduce.10.cloned.1.call-update
  176.9 0.0 all-reduce.12.cloned.1.call-start
  177.0 0.1 fusion.25
  177.1 0.1 reshape.50
  177.2 69.7 %all-reduce.10.cloned.1.call-done = f32[64,2,4,64]{3,2,1,0:T(4,128)} async-done(((f32[64,2,4,64]{3,2,1,0:T(4,128)}), f32[64,2,4,64]{3,2,1,0:T(4,128)}) %all-reduce.10.cloned.1.call-update) | async-done | bytes 131088 | tf_op jit(solution)/shard_map/psum | solution.py:75
  246.9 1.3 fusion.7
  248.2 0.1 convert_element_type.88
  248.3 0.8 convolution_convert_fusion.1
  249.2 0.0 all-reduce.12.cloned.1.call-update
  249.2 0.0 all-reduce.14.cloned.1.call-start
  249.2 30.8 %all-reduce.12.cloned.1.call-done = bf16[64,512]{1,0:T(8,128)(2,1)} async-done(((bf16[64,512]{1,0:T(8,128)(2,1)}), bf16[64,512]{1,0:T(8,128)(2,1)}) %all-reduce.12.cloned.1.call-update) | async-done | bytes 65552 | tf_op jit(solution)/shard_map/psum | solution.py:83
  280.1 4.1 %fusion.14 = f32[64,4096]{1,0:T(8,128)} fusion(bf16[512,4096]{1,0:T(8,128)(2,1)} %param.26, f32[512]{0:T(512)S(1)} %copy-done.7, bf16[64,512]{1,0:T(8,128)(2,1)S(1)} %copy-done.2, bf16[64,512]{1,0:T(8,128)(2,1)} %all-reduce.12.cloned.1.call-done), kind=kOutput, calls=%fused_computation.26 | convolution fusion | flops 268664832 | bytes 5376000 | tf_op jit(solution)/shard_map/dot_general | solution.py:89
  284.2 0.0 all-reduce.16.cloned.1.call-start
  284.3 0.1 fusion.11
  284.4 21.7 %psum.85 = f32[64]{0:T(128)S(1)} all-reduce(f32[64]{0:T(128)S(1)} %fusion.11), channel_id=1, replica_groups=mesh['kv'=8,'tp'=4] {'kv'}, use_global_device_ids=true, to_apply=%region_14.15 | all-reduce | flops 64 | bytes 512 | tf_op jit(solution)/shard_map/psum | solution.py:90
  306.1 56.6 %all-reduce.14.cloned.1.call-done = f32[64,4096]{1,0:T(8,128)} async-done(((f32[64,4096]{1,0:T(8,128)}), f32[64,4096]{1,0:T(8,128)}) %all-reduce.14.cloned.1.call-update) | async-done | bytes 1048592 | tf_op jit(solution)/shard_map/psum | solution.py:90
  362.8 4.0 convolution_convert_fusion
  366.8 0.0 all-reduce.16.cloned.1.call-update
  366.8 31.3 %all-reduce.16.cloned.1.call-done = bf16[64,512]{1,0:T(8,128)(2,1)} async-done(((bf16[64,512]{1,0:T(8,128)(2,1)}), bf16[64,512]{1,0:T(8,128)(2,1)}) %all-reduce.16.cloned.1.call-update) | async-done | bytes 65552 | tf_op jit(solution)/shard_map/psum | solution.py:94
  398.1 1.5 fusion.13
  (25 shorter events, 0.2 us)
Async XLA Ops:
  6.5 1.0 copy-start
  6.5 77.3 %all-reduce.8.cloned.1.call-start = ((), (), s32[]{:S(2)}) async-start(), calls=%async_computation | async-start | bytes 262144 | tf_op jit(solution)/shard_map/psum | solution.py:41
  9.3 237.6 %all-reduce.10.cloned.1.call-start = ((), (), s32[]{:S(2)}) async-start(), calls=%async_computation.1 | async-start | bytes 524288 | tf_op jit(solution)/shard_map/psum | solution.py:75
  51.9 2.2 copy-start.2
  51.9 2.2 copy-start.5
  51.9 2.2 copy-start.6
  51.9 33.5 %copy-start.8 = (f32[64]{0:T(128)S(1)}, f32[64]{0:T(128)}, u32[]{:S(2)}) copy-start(f32[64]{0:T(128)} %param.20) | copy-start | bytes 772
  95.1 72.8 %copy-start.1 = (f32[64,2,4,1024]{3,2,1,0:T(4,128)S(1)}, f32[64,2,4,1024]{3,2,1,0:T(4,128)}, u32[]{:S(2)}) copy-start(f32[64,2,4,1024]{3,2,1,0:T(4,128)} %get-tuple-element.15) | copy-start | bytes 6291460
  167.9 80.4 %copy-start.4 = (bf16[512,512]{1,0:T(8,128)(2,1)S(1)}, bf16[512,512]{1,0:T(8,128)(2,1)}, u32[]{:S(2)}) copy-start(bf16[512,512]{1,0:T(8,128)(2,1)} %param.24) | copy-start | bytes 1572868
  167.9 112.1 %copy-start.7 = (f32[512]{0:T(512)S(1)}, f32[512]{0:T(512)}, u32[]{:S(2)}) copy-start(f32[512]{0:T(512)} %param.25) | copy-start | bytes 6148
  176.9 103.1 %all-reduce.12.cloned.1.call-start = ((), (), s32[]{:S(2)}) async-start(), calls=%async_computation.2 | async-start | bytes 131072 | tf_op jit(solution)/shard_map/psum | solution.py:83
  249.2 113.6 %all-reduce.14.cloned.1.call-start = ((), (), s32[]{:S(2)}) async-start(), calls=%async_computation.3 | async-start | bytes 2097152 | tf_op jit(solution)/shard_map/psum | solution.py:90
  280.1 4.2 %copy-start.3 = (bf16[64,512]{1,0:T(8,128)(2,1)S(1)}, bf16[64,512]{1,0:T(8,128)(2,1)}, u32[]{:S(2)}) copy-start(bf16[64,512]{1,0:T(8,128)(2,1)} %all-reduce.12.cloned.1.call-done) | copy-start | bytes 196612
  284.2 113.9 %all-reduce.16.cloned.1.call-start = ((), (), s32[]{:S(2)}) async-start(), calls=%async_computation.4 | async-start | bytes 131072 | tf_op jit(solution)/shard_map/psum | solution.py:94
Sparse Core Ops, SparseCore 0:
  10.7 73.1 all-reduce.7
  177.1 69.7 all-reduce.9
  249.3 30.7 all-reduce.11
  284.4 78.3 all-reduce.13
  366.9 31.1 all-reduce.15
where the time goes:
time: 407 us; the launch traced here: 406 us
  waiting for transfers between devices  218 us (54%)
  blocking collectives  131 us (32%)
  matrix products  31.7 us (8%)
  between operations  13.4 us (3%)
  other arithmetic  8.11 us (2%)
    psum x1, waiting for transfers between devices, shards(): lax.psum((jnp.sum(weights, axis=-1), partial_values), 'kv')  69.7 us
    psum x1, waiting for transfers between devices, shards(): up_full, total_mlp = lax.psum((up_terms, squares_mlp), 'kv')  56.6 us
    psum x1, blocking collectives, shards(): lax.psum((query_terms, key_terms, value_terms, forget_terms, squares_mix)...  39.3 us
    pmax x1, blocking collectives, shards(): peak_score = jnp.maximum(lax.pmax(local_peak, 'kv'), own_score)  35.9 us
    psum x1, blocking collectives, shards(): lax.psum((jnp.sum(weights, axis=-1), partial_values), 'kv')  33.9 us
    psum x1, waiting for transfers between devices, shards(): mlp_out = lax.psum(down_terms.astype(jnp.bfloat16), 'tp')  31.3 us
    psum x1, waiting for transfers between devices, shards(): attn_out = lax.psum(attn_terms.astype(jnp.bfloat16), 'tp')  30.8 us
    psum x1, waiting for transfers between devices, shards(): lax.psum((query_terms, key_terms, value_terms, forget_terms, squares_mix)...  29.6 us
  transfers between devices with their start and end apart: 5, of which 5 were waited for; matrix products, arithmetic and copies ran while one was open for 1% of the time, Pallas kernels for 0%

commit v1 on v0

v1 whole, which is shorter than its diff:
```python
import functools

import jax
import jax.numpy as jnp
from jax import lax
from jax.experimental import pallas as pl
from jax.experimental.pallas import tpu as pltpu
from jax.sharding import PartitionSpec as P

MESH = pl.DeviceIdType.MESH
HEAD_DIM = 64
EPS = 1e-06
F32 = jnp.float32
BF16 = jnp.bfloat16


def greet(n, t, with_tp):
    kv, tp = lax.axis_index("kv"), lax.axis_index("tp")
    barrier = pltpu.get_barrier_semaphore()
    count = n - 1
    for i in range(1, n):
        pl.semaphore_signal(
            barrier, inc=1, device_id=(lax.rem(kv + i, n), tp), device_id_type=MESH
        )
    if with_tp:
        count += t - 1
        for i in range(1, t):
            pl.semaphore_signal(
                barrier, inc=1, device_id=(kv, lax.rem(tp + i, t)), device_id_type=MESH
            )
    pl.semaphore_wait(barrier, count)


def remote(src, dst, send, recv, kv, tp):
    return pltpu.make_async_remote_copy(
        src_ref=src,
        dst_ref=dst,
        send_sem=send,
        recv_sem=recv,
        device_id=(kv, tp),
        device_id_type=MESH,
    )


def project_kernel(
    n, t, d, tok, gain, wq, wk, wv, wf, qgain, out, parts, got, mine, ssem, rsem, asem, bsem
):
    kv, tp = lax.axis_index("kv"), lax.axis_index("tp")
    greet(n, t, False)
    rows = tok.shape[0]
    rc = rows // n
    nq, nk, nf = wq.shape[1], wk.shape[1], wf.shape[1]
    stream = tok[...].astype(F32)
    squares = jnp.sum(stream * stream, axis=1, keepdims=True)
    normed = (stream * gain[...]).astype(BF16)
    q = jnp.dot(normed, wq[...], preferred_element_type=F32)
    k = jnp.dot(normed, wk[...], preferred_element_type=F32)
    v = jnp.dot(normed, wv[...], preferred_element_type=F32)
    f = jnp.dot(normed, wf[...], preferred_element_type=F32)
    for p in range(n):
        cut = slice(p * rc, (p + 1) * rc)
        parts[p, :, 0:nq] = q[cut]
        parts[p, :, nq : nq + nk] = k[cut]
        parts[p, :, nq + nk : nq + 2 * nk] = v[cut]
        base = nq + 2 * nk
        parts[p, :, base : base + 128] = jnp.broadcast_to(squares[cut], (rc, 128))
        parts[p, :, base : base + nf] = f[cut]
    sends = []
    for i in range(1, n):
        peer = lax.rem(kv + i, n)
        c = remote(parts.at[peer], got.at[i], ssem.at[i], rsem.at[i], peer, tp)
        c.start()
        sends.append(c)
    total = parts[kv]
    for c in sends:
        c.wait_recv()
    for i in range(1, n):
        total = total + got[i]
    base = nq + 2 * nk
    scale = lax.rsqrt(total[:, base + 127 : base + 128] / d + EPS)
    scaled = total * scale
    raw = scaled[:, 0:nq]
    raw2 = raw * raw
    head = lax.broadcasted_iota(jnp.int32, raw.shape, 1) // HEAD_DIM
    inverse = jnp.zeros_like(raw)
    for h in range(nq // HEAD_DIM):
        on = head == h
        mean = jnp.sum(jnp.where(on, raw2, 0.0), axis=1, keepdims=True) / HEAD_DIM
        inverse = jnp.where(on, lax.rsqrt(mean + EPS), inverse)
    mine[:, 0:nq] = raw * inverse * qgain[...]
    mine[:, nq:base] = scaled[:, nq:base]
    gate = scaled[:, base:]
    mine[:, base:] = jnp.minimum(gate, 0.0) - jnp.log1p(jnp.exp(-jnp.abs(gate)))
    gathers = []
    for i in range(1, n):
        peer = lax.rem(kv + i, n)
        c = remote(mine, out.at[kv], asem.at[i], bsem.at[i], peer, tp)
        c.start()
        gathers.append(c)
    out[kv] = mine[...]
    for i in range(1, n):
        gathers[i - 1].wait_recv()
    for c in sends + gathers:
        c.wait_send()


def attend_kernel(sharing, q_ref, k_ref, v_ref, d_ref, o_ref):
    steps, heads, _ = q_ref.shape
    groups = heads // sharing
    row = lax.broadcasted_iota(jnp.int32, (heads, HEAD_DIM), 0) // sharing
    for i in range(steps):
        s = jnp.dot(q_ref[i], k_ref[i], preferred_element_type=F32) * (HEAD_DIM**-0.5)
        s = s + d_ref[i]
        m = jnp.max(s, axis=1, keepdims=True)
        w = jnp.exp(s - m)
        l = jnp.sum(w, axis=1, keepdims=True)
        o = lax.dot_general(
            w.astype(BF16), v_ref[i], (((1,), (1,)), ((), ())), preferred_element_type=F32
        )
        picked = o[:, 0:HEAD_DIM]
        for g in range(1, groups):
            picked = jnp.where(row == g, o[:, g * HEAD_DIM : (g + 1) * HEAD_DIM], picked)
        o_ref[i, :, 0:64] = picked
        o_ref[i, :, 64:96] = jnp.broadcast_to(m, (heads, 32))
        o_ref[i, :, 96:128] = jnp.broadcast_to(l, (heads, 32))


def rest_kernel(
    n, t, d, packed, own, tok, gain, wo_hbm, wu_hbm, wd_hbm, out,
    wo, wu, wd, got, att, allatt, full, tpa, tpb, upsend, upgot, sqs, sqgot, hid,
    wsem, sem, tsem,
):
    kv, tp = lax.axis_index("kv"), lax.axis_index("tp")
    loads = [
        pltpu.make_async_copy(a, b, wsem.at[j])
        for j, (a, b) in enumerate(((wo_hbm, wo), (wu_hbm, wu), (wd_hbm, wd)))
    ]
    for c in loads:
        c.start()
    greet(n, t, True)
    rows, heads, _ = packed.shape
    rc = rows // n
    ffc = wu.shape[1] // n
    started = []

    def send(kind, i, src, dst):
        peer = lax.rem(kv + i, n)
        c = remote(src(peer), dst, sem.at[2 * kind, i], sem.at[2 * kind + 1, i], peer, tp)
        c.start()
        started.append(c)
        return c

    def tp_sum(kind, buf, value):
        buf[tp] = value.astype(BF16)
        copies = []
        for i in range(1, t):
            c = remote(
                buf.at[tp], buf.at[tp], tsem.at[2 * kind, i], tsem.at[2 * kind + 1, i],
                kv, lax.rem(tp + i, t),
            )
            c.start()
            copies.append(c)
            started.append(c)
        for c in copies:
            c.wait_recv()
        total = buf[0].astype(F32)
        for j in range(1, t):
            total = total + buf[j].astype(F32)
        return total.astype(BF16).astype(F32)

    copies = [
        send(0, i, lambda p: packed.at[pl.ds(p * rc, rc)], got.at[i]) for i in range(1, n)
    ]
    mine = packed[pl.ds(kv * rc, rc)]
    extra = own[pl.ds(kv * rc, rc)]
    own_score = extra[:, :, 64:65]
    forget = extra[:, :, 96:97]
    for c in copies:
        c.wait_recv()
    blocks = [mine] + [got[i] for i in range(1, n)]
    peaks = [b[:, :, 64:65] + forget for b in blocks]
    peak = own_score
    for p in peaks:
        peak = jnp.maximum(peak, p)
    own_weight = jnp.exp(own_score - peak)
    mass = own_weight
    summed = own_weight.astype(BF16).astype(F32) * extra[:, :, 0:64]
    for b, p in zip(blocks, peaks):
        w = jnp.exp(p - peak)
        mass = mass + w * b[:, :, 96:97]
        summed = summed + w * b[:, :, 0:64]
    head = summed / mass
    for h in range(heads):
        att[:, h * HEAD_DIM : (h + 1) * HEAD_DIM] = head[:, h, :].astype(BF16)
    copies = [send(1, i, lambda p: att, allatt.at[kv]) for i in range(1, n)]
    allatt[kv] = att[...]
    loads[0].wait()
    for c in copies:
        c.wait_recv()
    for p in range(n):
        full[p * rc : (p + 1) * rc, :] = allatt[p].astype(F32)
    attn = jnp.dot(full[...].astype(BF16), wo[...], preferred_element_type=F32)
    attn = tp_sum(0, tpa, attn)
    residual = (tok[...].astype(F32) + attn).astype(BF16).astype(F32)
    normed = (residual * gain[...]).astype(BF16)
    loads[1].wait()
    copies = []
    for i in list(range(1, n)) + [0]:
        peer = lax.rem(kv + i, n)
        cols = pl.ds(pl.multiple_of(peer * ffc, ffc), ffc)
        part = jnp.dot(normed, wu[:, cols], preferred_element_type=F32)
        if i:
            upsend[i] = part.astype(BF16)
            copies.append(send(2, i, lambda p: upsend.at[i], upgot.at[i]))
    sqs[...] = lax.dot_general(
        jnp.ones((8, residual.shape[1]), F32),
        residual * residual,
        (((1,), (1,)), ((), ())),
        preferred_element_type=F32,
        precision=lax.Precision.HIGHEST,
    )
    sq_copies = [send(3, i, lambda p: sqs, sqgot.at[i]) for i in range(1, n)]
    total = sqs[...]
    for i in range(1, n):
        sq_copies[i - 1].wait_recv()
        total = total + sqgot[i]
    r = lax.broadcasted_iota(jnp.int32, (rows, rows), 0)
    c_ = lax.broadcasted_iota(jnp.int32, (rows, rows), 1)
    wide = jnp.broadcast_to(total[0:1, :], (rows, rows))
    column = jnp.sum(jnp.where(r == c_, wide, 0.0), axis=1, keepdims=True)
    scale = lax.rsqrt(column / d + EPS)
    for i in range(1, n):
        copies[i - 1].wait_recv()
        part = part + upgot[i].astype(F32)
    hidden = jnp.square(jnp.maximum(part * scale, 0.0)).astype(BF16)
    hid[kv] = hidden
    copies = [send(4, i, lambda p: hid.at[kv], hid.at[kv]) for i in range(1, n)]
    loads[2].wait()
    here = pl.ds(pl.multiple_of(kv * ffc, ffc), ffc)
    down = jnp.dot(hidden, wd[here, :], preferred_element_type=F32)
    for i in range(1, n):
        src = lax.rem(kv + n - i, n)
        copies[i - 1].wait_recv()
        there = pl.ds(pl.multiple_of(src * ffc, ffc), ffc)
        down = down + jnp.dot(hid[src], wd[there, :], preferred_element_type=F32)
    mlp = tp_sum(1, tpb, down)
    out[...] = (residual + mlp).astype(BF16)
    for c in started:
        c.wait_send()


def shards(
    n, t, tokens, mix_gain, w_query, w_key, w_value, w_forget, query_gain,
    key_cache, value_cache, decay_cache, w_out, mlp_gain, w_up, w_down,
):
    rows, dl = tokens.shape
    d = dl * n
    rc = rows // n
    heads = w_forget.shape[1]
    groups = key_cache.shape[1]
    sharing = heads // groups
    nq, nk = w_query.shape[1], w_key.shape[1]
    span = key_cache.shape[3]
    vmem = pl.BlockSpec(memory_space=pltpu.VMEM)
    anywhere = pl.BlockSpec(memory_space=pl.ANY)
    nk_pad = nk
    width = nq + 2 * nk_pad + 128
    dma = pltpu.SemaphoreType.DMA
    proj = pl.pallas_call(
        functools.partial(project_kernel, n, t, d),
        out_shape=jax.ShapeDtypeStruct((n, rc, width), F32),
        in_specs=[vmem] * 7,
        out_specs=vmem,
        scratch_shapes=[
            pltpu.VMEM((n, rc, width), F32),
            pltpu.VMEM((n, rc, width), F32),
            pltpu.VMEM((rc, width), F32),
            dma((n,)), dma((n,)), dma((n,)), dma((n,)),
        ],
        compiler_params=pltpu.CompilerParams(collective_id=0, has_side_effects=True),
    )(
        tokens, mix_gain[None, :], w_query, w_key, w_value, w_forget,
        jnp.tile(query_gain, heads)[None, :],
    ).reshape(rows, width)
    query = proj[:, :nq].astype(BF16).reshape(rows, groups, sharing, HEAD_DIM)
    key_new = proj[:, nq : nq + nk].astype(BF16).reshape(rows, groups, HEAD_DIM)
    value_new = proj[:, nq + nk : nq + 2 * nk].astype(BF16).astype(F32)
    value_new = value_new.reshape(rows, groups, 1, HEAD_DIM)
    forget = proj[:, nq + 2 * nk : nq + 2 * nk + heads].reshape(rows, heads, 1)
    own_score = jnp.sum(
        query.astype(F32) * key_new.astype(F32)[:, :, None, :], axis=-1
    ) * (HEAD_DIM**-0.5)
    own = jnp.concatenate(
        [
            jnp.broadcast_to(value_new, (rows, groups, sharing, HEAD_DIM)).reshape(
                rows, heads, HEAD_DIM
            ),
            jnp.broadcast_to(own_score.reshape(rows, heads, 1), (rows, heads, 32)),
            jnp.broadcast_to(forget, (rows, heads, 32)),
        ],
        axis=-1,
    )
    same = jnp.eye(groups, dtype=jnp.bool_)[None, :, None, :, None]
    spread = jnp.where(same, query[:, :, :, None, :], jnp.zeros((), BF16))
    spread = spread.reshape(rows, heads, groups * HEAD_DIM)
    step = 8
    block = lambda a, b: pl.BlockSpec((step, a, b), lambda i: (i, 0, 0))
    gd = groups * HEAD_DIM
    packed = pl.pallas_call(
        functools.partial(attend_kernel, sharing),
        grid=(rows // step,),
        out_shape=jax.ShapeDtypeStruct((rows, heads, 128), F32),
        in_specs=[block(heads, gd), block(gd, span), block(gd, span), block(heads, span)],
        out_specs=block(heads, 128),
    )(
        spread,
        key_cache.reshape(rows, gd, span),
        value_cache.reshape(rows, gd, span),
        decay_cache,
    )
    ff = w_up.shape[1]
    ffc = ff // n
    return pl.pallas_call(
        functools.partial(rest_kernel, n, t, d),
        out_shape=jax.ShapeDtypeStruct((rows, dl), BF16),
        in_specs=[vmem] * 4 + [anywhere] * 3,
        out_specs=vmem,
        scratch_shapes=[
            pltpu.VMEM(w_out.shape, BF16),
            pltpu.VMEM(w_up.shape, BF16),
            pltpu.VMEM(w_down.shape, BF16),
            pltpu.VMEM((n, rc, heads, 128), F32),
            pltpu.VMEM((rc, nq), BF16),
            pltpu.VMEM((n, rc, nq), BF16),
            pltpu.VMEM((rows, nq), F32),
            pltpu.VMEM((t, rows, dl), BF16),
            pltpu.VMEM((t, rows, dl), BF16),
            pltpu.VMEM((n, rows, ffc), BF16),
            pltpu.VMEM((n, rows, ffc), BF16),
            pltpu.VMEM((8, rows), F32),
            pltpu.VMEM((n, 8, rows), F32),
            pltpu.VMEM((n, rows, ffc), BF16),
            dma((3,)), dma((10, n)), dma((4, t)),
        ],
        compiler_params=pltpu.CompilerParams(collective_id=1, has_side_effects=True),
    )(packed, own, tokens, mlp_gain[None, :], w_out, w_up, w_down)


def solution(mesh):
    in_specs = (
        P(None, "kv"),
        P("kv"),
        P("kv", "tp"),
        P("kv", "tp"),
        P("kv", "tp"),
        P("kv", "tp"),
        P(),
        P(None, "tp", None, "kv"),
        P(None, "tp", None, "kv"),
        P(None, "tp", "kv"),
        P("tp", "kv"),
        P("kv"),
        P("kv", "tp"),
        P("tp", "kv"),
    )
    body = functools.partial(shards, mesh.shape["kv"], mesh.shape["tp"])
    return jax.shard_map(
        body, mesh=mesh, in_specs=in_specs, out_specs=P(None, "kv"), check_vma=False
    )
```

time: 407 us -> 101 us (0.25)
  waiting for transfers between devices: 218 us -> 0 us
  blocking collectives: 131 us -> 0 us
  Pallas kernels: 0 us -> 91.2 us
  matrix products: 31.7 us -> 0 us
  between operations: 13.4 us -> 0.1 us
  other arithmetic: 8.11 us -> 2.82 us
    psum x5 -> x0, waiting for transfers between devices: 218 us -> none  [the longest x1 69.7 us: shards(): lax.psum((jnp.sum(weights, axis=-1), partial_values), 'kv')]
    psum x3 -> x0, blocking collectives: 94.8 us -> none  [the longest x1 39.3 us: shards(): lax.psum((query_terms, key_terms, value_terms, forget_terms, squares_mix)...]
    pallas_call x0 -> x3, Pallas kernels: none -> 91.2 us  [the longest x1 52.7 us: shards(): pl.pallas_call(functools.partial(rest_kernel, n, t, d), out_shape=jax.Sha...]
    pmax x1 -> x0, blocking collectives: 35.9 us -> none  [shards(): peak_score = jnp.maximum(lax.pmax(local_peak, 'kv'), own_score)]
    dot_general x10 -> x0, matrix products: 31.7 us -> none  [the longest x1 9.45 us: shards(): jnp.einsum('bgjd,bgdp->bgjp', query, key_cache, preferred_element_type=jn...]
  transfers between devices with their start and end apart: 5 -> 0, of which waited for: 5 -> 0; matrix products, arithmetic and copies ran while one was open for 1% -> 0% of each run, Pallas kernels for 0% -> 0%
where the time goes in v1:
time: 101 us; the launch traced here: 100 us
  Pallas kernels  91.2 us (90%)
  local copies, waits for them, and re-layouts  6.32 us (6%)
  other arithmetic  2.82 us (3%)
    pallas_call x1, Pallas kernels, shards(): pl.pallas_call(functools.partial(rest_kernel, n, t, d), out_shape=jax.Sha...  52.7 us
    pallas_call x1, Pallas kernels, shards(): pl.pallas_call(functools.partial(project_kernel, n, t, d), out_shape=jax....  19.8 us
    pallas_call x1, Pallas kernels, shards(): pl.pallas_call(functools.partial(attend_kernel, sharing), grid=(rows // s...  18.7 us
    unnamed x2, local copies, waits for them, and re-layouts  2.96 us

profile of v1, /device:TPU:0, one launch (start us, length us, event | category | flops | bytes accessed | tf_op | source)
XLA Modules:
  0.0 100.4 jit_solution(11801931442827316576)
XLA Ops:
  0.0 1.5 %copy.21.wf = bf16[512,8]{1,0:T(8,128)(2,1)} copy(bf16[512,8]{0,1:T(8,128)(2,1)} %param.19) | data formatting | bytes 16384 | tf_op args[5]
  1.5 0.7 tile.2
  2.1 0.7 broadcast_in_dim_tile.3.qgain
  2.8 19.8 %shard_map.136 = f32[8,8,896]{2,1,0:T(8,128)} custom-call(bf16[64,512]{1,0:T(8,128)(2,1)} %tok.3, f32[1,512]{1,0:T(1,128)} %bitcast.13, bf16[512,512]{1,0:T(8,128)(2,1)} %wq.1, bf16[512,128]{1,0:T(8,128)(2,1)} %wk.1, bf16[512,128]{1,0:T(8,128)(2,1)} %wv.1, bf16[512,8]{1,0:T(8,128)(2,1)} %copy.21.wf, f32[1,512]{1,0:T(1,128)} %broadcast_in_dim_tile.3.qgain), custom_call_target="tpu_custom_call" | custom-call | tf_op jit(solution)/shard_map/pallas_call | solution.py:269
  22.6 1.0 bitcast_convert_fusion
  23.6 0.1 broadcast_in_dim.60
  23.8 0.1 reshape.50
  23.9 0.3 multiply_reduce_fusion
  24.1 0.1 copy.22
  24.2 0.1 copy.23
  24.3 0.1 broadcast_in_dim.67
  24.5 0.1 reshape.49
  24.6 0.8 slice.22
  25.4 0.1 broadcast_in_dim.68
  25.5 0.9 pad_maximum_fusion.own
  26.4 0.2 broadcast_in_dim.61
  26.6 0.1 broadcast_in_dim.62
  26.8 0.1 broadcast_in_dim.56
  26.8 0.1 broadcast_in_dim.57
  26.9 0.7 broadcast_select_fusion.q_ref
  27.6 18.7 %shard_map.137.packed = f32[64,8,128]{2,1,0:T(8,128)} custom-call(bf16[64,8,128]{2,1,0:T(8,128)(2,1)} %broadcast_select_fusion.q_ref, bf16[64,128,1024]{2,1,0:T(8,128)(2,1)} %bitcast.8, bf16[64,128,1024]{2,1,0:T(8,128)(2,1)} %bitcast.9, f32[64,8,1024]{2,1,0:T(8,128)} %d_ref.1), custom_call_target="tpu_custom_call" | custom-call | tf_op jit(solution)/shard_map/pallas_call | solution.py:309
  46.3 52.7 %shard_map.138 = bf16[64,512]{1,0:T(8,128)(2,1)} custom-call(f32[64,8,128]{2,1,0:T(8,128)} %shard_map.137.packed, f32[64,8,128]{2,1,0:T(8,128)} %pad_maximum_fusion.own, bf16[64,512]{1,0:T(8,128)(2,1)} %tok.3, f32[1,512]{1,0:T(1,128)} %bitcast.14, bf16[512,512]{1,0:T(8,128)(2,1)} %wo_hbm.1, bf16[512,4096]{1,0:T(8,128)(2,1)} %wu_hbm.1, bf16[4096,512]{1,0:T(8,128)(2,1)} %wd_hbm.1), custom_call_target="tpu_custom_call" | custom-call | tf_op jit(solution)/shard_map/pallas_call | solution.py:323
  99.0 1.5 %copy.25 = bf16[64,512]{1,0:T(8,128)(2,1)} copy(bf16[64,512]{1,0:T(8,128)(2,1)} %shard_map.138) | data formatting | bytes 131072
  (5 shorter events, 0.1 us)

commit v2 on v1

--- a/solution.py
+++ b/solution.py
@@ -49,14 +49,16 @@
     greet(n, t, False)
     rows = tok.shape[0]
     rc = rows // n
-    nq, nk, nf = wq.shape[1], wk.shape[1], wf.shape[1]
+    nq, nk, nf = wq.shape[1], wk.shape[1], wf.shape[0]
     stream = tok[...].astype(F32)
     squares = jnp.sum(stream * stream, axis=1, keepdims=True)
     normed = (stream * gain[...]).astype(BF16)
     q = jnp.dot(normed, wq[...], preferred_element_type=F32)
     k = jnp.dot(normed, wk[...], preferred_element_type=F32)
     v = jnp.dot(normed, wv[...], preferred_element_type=F32)
-    f = jnp.dot(normed, wf[...], preferred_element_type=F32)
+    f = lax.dot_general(
+        normed, wf[...], (((1,), (1,)), ((), ())), preferred_element_type=F32
+    )
     for p in range(n):
         cut = slice(p * rc, (p + 1) * rc)
         parts[p, :, 0:nq] = q[cut]
@@ -87,7 +89,8 @@
         on = head == h
         mean = jnp.sum(jnp.where(on, raw2, 0.0), axis=1, keepdims=True) / HEAD_DIM
         inverse = jnp.where(on, lax.rsqrt(mean + EPS), inverse)
-    mine[:, 0:nq] = raw * inverse * qgain[...]
+    gains = jnp.concatenate([qgain[...]] * (nq // HEAD_DIM), axis=1)
+    mine[:, 0:nq] = raw * inverse * gains
     mine[:, nq:base] = scaled[:, nq:base]
     gate = scaled[:, base:]
     mine[:, base:] = jnp.minimum(gate, 0.0) - jnp.log1p(jnp.exp(-jnp.abs(gate)))
@@ -108,26 +111,32 @@
     steps, heads, _ = q_ref.shape
     groups = heads // sharing
     row = lax.broadcasted_iota(jnp.int32, (heads, HEAD_DIM), 0) // sharing
-    for i in range(steps):
-        s = jnp.dot(q_ref[i], k_ref[i], preferred_element_type=F32) * (HEAD_DIM**-0.5)
-        s = s + d_ref[i]
-        m = jnp.max(s, axis=1, keepdims=True)
-        w = jnp.exp(s - m)
-        l = jnp.sum(w, axis=1, keepdims=True)
-        o = lax.dot_general(
+    scores = [
+        jnp.dot(q_ref[i], k_ref[i], preferred_element_type=F32) * (HEAD_DIM**-0.5) + d_ref[i]
+        for i in range(steps)
+    ]
+    peaks = [jnp.max(s, axis=1, keepdims=True) for s in scores]
+    weights = [jnp.exp(s - m) for s, m in zip(scores, peaks)]
+    sums = [jnp.sum(w, axis=1, keepdims=True) for w in weights]
+    outs = [
+        lax.dot_general(
             w.astype(BF16), v_ref[i], (((1,), (1,)), ((), ())), preferred_element_type=F32
         )
+        for i, w in enumerate(weights)
+    ]
+    for i in range(steps):
+        o = outs[i]
         picked = o[:, 0:HEAD_DIM]
         for g in range(1, groups):
             picked = jnp.where(row == g, o[:, g * HEAD_DIM : (g + 1) * HEAD_DIM], picked)
         o_ref[i, :, 0:64] = picked
-        o_ref[i, :, 64:96] = jnp.broadcast_to(m, (heads, 32))
-        o_ref[i, :, 96:128] = jnp.broadcast_to(l, (heads, 32))
+        o_ref[i, :, 64:96] = jnp.broadcast_to(peaks[i], (heads, 32))
+        o_ref[i, :, 96:128] = jnp.broadcast_to(sums[i], (heads, 32))
 
 
 def rest_kernel(
     n, t, d, packed, own, tok, gain, wo_hbm, wu_hbm, wd_hbm, out,
-    wo, wu, wd, got, att, allatt, full, tpa, tpb, upsend, upgot, sqs, sqgot, hid,
+    wo, wu, wd, got, att, allatt, full, tpa, tpb, upsend, upgot, upsend2, upgot2, keep, sqs, sqgot, hid,
     wsem, sem, tsem,
 ):
     kv, tp = lax.axis_index("kv"), lax.axis_index("tp")
@@ -143,8 +152,9 @@
     ffc = wu.shape[1] // n
     started = []
 
-    def send(kind, i, src, dst):
-        peer = lax.rem(kv + i, n)
+    def send(kind, i, src, dst, peer=None):
+        if peer is None:
+            peer = lax.rem(kv + i, n)
         c = remote(src(peer), dst, sem.at[2 * kind, i], sem.at[2 * kind + 1, i], peer, tp)
         c.start()
         started.append(c)
@@ -204,14 +214,22 @@
     residual = (tok[...].astype(F32) + attn).astype(BF16).astype(F32)
     normed = (residual * gain[...]).astype(BF16)
     loads[1].wait()
-    copies = []
-    for i in list(range(1, n)) + [0]:
-        peer = lax.rem(kv + i, n)
-        cols = pl.ds(pl.multiple_of(peer * ffc, ffc), ffc)
-        part = jnp.dot(normed, wu[:, cols], preferred_element_type=F32)
-        if i:
-            upsend[i] = part.astype(BF16)
-            copies.append(send(2, i, lambda p: upsend.at[i], upgot.at[i]))
+    half = n // 2
+    side = lax.rem(kv, 2)
+    place = kv // 2
+    partner = kv + 1 - 2 * side
+    order = list(range(1, half)) + [0]
+
+    def term(dest):
+        cols = pl.ds(pl.multiple_of(dest * ffc, ffc), ffc)
+        return jnp.dot(normed, wu[:, cols], preferred_element_type=F32)
+
+    firsts = {}
+    for j in order:
+        upsend[j] = term(2 * lax.rem(place + j, half) + 1 - side).astype(BF16)
+        firsts[j] = send(2, j, lambda p: upsend.at[j], upgot.at[j], partner)
+    for j in order:
+        keep[j] = term(2 * lax.rem(place + j, half) + side)
     sqs[...] = lax.dot_general(
         jnp.ones((8, residual.shape[1]), F32),
         residual * residual,
@@ -220,6 +238,15 @@
         precision=lax.Precision.HIGHEST,
     )
     sq_copies = [send(3, i, lambda p: sqs, sqgot.at[i]) for i in range(1, n)]
+    seconds = {}
+    for j in order:
+        firsts[j].wait_recv()
+        part = keep[j] + upgot[j].astype(F32)
+        if j:
+            upsend2[j] = part.astype(BF16)
+            seconds[j] = send(
+                4, j, lambda p: upsend2.at[j], upgot2.at[j], 2 * lax.rem(place + j, half) + side
+            )
     total = sqs[...]
     for i in range(1, n):
         sq_copies[i - 1].wait_recv()
@@ -229,20 +256,32 @@
     wide = jnp.broadcast_to(total[0:1, :], (rows, rows))
     column = jnp.sum(jnp.where(r == c_, wide, 0.0), axis=1, keepdims=True)
     scale = lax.rsqrt(column / d + EPS)
-    for i in range(1, n):
-        copies[i - 1].wait_recv()
-        part = part + upgot[i].astype(F32)
+    for j in range(1, half):
+        seconds[j].wait_recv()
+        part = part + upgot2[j].astype(F32)
     hidden = jnp.square(jnp.maximum(part * scale, 0.0)).astype(BF16)
     hid[kv] = hidden
-    copies = [send(4, i, lambda p: hid.at[kv], hid.at[kv]) for i in range(1, n)]
+    across = {0: send(6, 0, lambda p: hid.at[kv], hid.at[kv], partner)}
+    along = {}
+    for j in range(1, half):
+        along[j] = send(
+            5, j, lambda p: hid.at[kv], hid.at[kv], 2 * lax.rem(place + j, half) + side
+        )
     loads[2].wait()
-    here = pl.ds(pl.multiple_of(kv * ffc, ffc), ffc)
-    down = jnp.dot(hidden, wd[here, :], preferred_element_type=F32)
-    for i in range(1, n):
-        src = lax.rem(kv + n - i, n)
-        copies[i - 1].wait_recv()
+
+    def lower(src):
         there = pl.ds(pl.multiple_of(src * ffc, ffc), ffc)
-        down = down + jnp.dot(hid[src], wd[there, :], preferred_element_type=F32)
+        return jnp.dot(hid[src], wd[there, :], preferred_element_type=F32)
+
+    down = lower(kv)
+    for j in range(1, half):
+        src = 2 * lax.rem(place + half - j, half) + side
+        along[j].wait_recv()
+        across[j] = send(6, j, lambda p: hid.at[src], hid.at[src], partner)
+        down = down + lower(src)
+    for j in range(half):
+        across[j].wait_recv()
+        down = down + lower(2 * lax.rem(place + half - j, half) + 1 - side)
     mlp = tp_sum(1, tpb, down)
     out[...] = (residual + mlp).astype(BF16)
     for c in started:
@@ -279,8 +318,7 @@
         ],
         compiler_params=pltpu.CompilerParams(collective_id=0, has_side_effects=True),
     )(
-        tokens, mix_gain[None, :], w_query, w_key, w_value, w_forget,
-        jnp.tile(query_gain, heads)[None, :],
+        tokens, mix_gain[None, :], w_query, w_key, w_value, w_forget.T, query_gain[None, :],
     ).reshape(rows, width)
     query = proj[:, :nq].astype(BF16).reshape(rows, groups, sharing, HEAD_DIM)
     key_new = proj[:, nq : nq + nk].astype(BF16).reshape(rows, groups, HEAD_DIM)
@@ -335,12 +373,15 @@
             pltpu.VMEM((rows, nq), F32),
             pltpu.VMEM((t, rows, dl), BF16),
             pltpu.VMEM((t, rows, dl), BF16),
-            pltpu.VMEM((n, rows, ffc), BF16),
-            pltpu.VMEM((n, rows, ffc), BF16),
+            pltpu.VMEM((n // 2, rows, ffc), BF16),
+            pltpu.VMEM((n // 2, rows, ffc), BF16),
+            pltpu.VMEM((n // 2, rows, ffc), BF16),
+            pltpu.VMEM((n // 2, rows, ffc), BF16),
+            pltpu.VMEM((n // 2, rows, ffc), F32),
             pltpu.VMEM((8, rows), F32),
             pltpu.VMEM((n, 8, rows), F32),
             pltpu.VMEM((n, rows, ffc), BF16),
-            dma((3,)), dma((10, n)), dma((4, t)),
+            dma((3,)), dma((14, n)), dma((4, t)),
         ],
         compiler_params=pltpu.CompilerParams(collective_id=1, has_side_effects=True),
     )(packed, own, tokens, mlp_gain[None, :], w_out, w_up, w_down)

time: 101 us -> 90.3 us (0.89)
  Pallas kernels: 91.2 us -> 83.5 us
  local copies, waits for them, and re-layouts: 6.32 us -> 3.53 us
    pallas_call x1, Pallas kernels: 52.7 us -> 47.9 us  [shards(): pl.pallas_call(functools.partial(rest_kernel, n, t, d), out_shape=jax.Sha...]
    pallas_call x1, Pallas kernels: 18.7 us -> 15.8 us  [shards(): pl.pallas_call(functools.partial(attend_kernel, sharing), grid=(rows // s...]
    unnamed x2 -> x1, local copies, waits for them, and re-layouts: 2.96 us -> 1.47 us
    another operation x2 -> x0, local copies, waits for them, and re-layouts: 1.31 us -> none  [shards(): jnp.tile(query_gain, heads)[None, :]]
where the time goes in v2:
time: 90.3 us; the launch traced here: 90 us
  Pallas kernels  83.5 us (92%)
  local copies, waits for them, and re-layouts  3.53 us (4%)
  other arithmetic  2.82 us (3%)
    pallas_call x1, Pallas kernels, shards(): pl.pallas_call(functools.partial(rest_kernel, n, t, d), out_shape=jax.Sha...  47.9 us
    pallas_call x1, Pallas kernels, shards(): pl.pallas_call(functools.partial(project_kernel, n, t, d), out_shape=jax....  19.8 us
    pallas_call x1, Pallas kernels, shards(): pl.pallas_call(functools.partial(attend_kernel, sharing), grid=(rows // s...  15.8 us

profile of v2, /device:TPU:0, one launch (start us, length us, event | category | flops | bytes accessed | tf_op | source)
XLA Modules:
  0.0 90.0 jit_solution(856469708680988134)
XLA Ops:
  0.0 19.8 %shard_map.136 = f32[8,8,896]{2,1,0:T(8,128)} custom-call(bf16[64,512]{1,0:T(8,128)(2,1)} %tok.3, f32[1,512]{1,0:T(1,128)} %bitcast.16, bf16[512,512]{1,0:T(8,128)(2,1)} %wq.1, bf16[512,128]{1,0:T(8,128)(2,1)} %wk.1, bf16[512,128]{1,0:T(8,128)(2,1)} %wv.1, bf16[8,512]{1,0:T(8,128)(2,1)} %bitcast.15, f32[1,64]{1,0:T(1,128)} %bitcast.18), custom_call_target="tpu_custom_call" | custom-call | tf_op jit(solution)/shard_map/pallas_call | solution.py:308
  19.8 1.0 %bitcast_convert_fusion = bf16[64,896]{1,0:T(8,128)(2,1)S(1)} fusion(f32[8,8,896]{2,1,0:T(8,128)} %shard_map.136), kind=kLoop, calls=%fused_computation.7 | loop fusion | flops 57344 | bytes 344064 | tf_op jit(solution)/shard_map/convert.4
  20.8 0.1 broadcast_in_dim.64
  20.9 0.1 reshape.49
  21.0 0.3 multiply_reduce_fusion
  21.3 0.1 copy.18
  21.4 0.1 copy.19
  21.5 0.1 broadcast_in_dim.71
  21.6 0.1 reshape.48
  21.8 0.8 slice.22
  22.5 0.1 broadcast_in_dim.72
  22.7 0.9 %pad_maximum_fusion.own = f32[64,8,128]{2,1,0:T(8,128)} fusion(f32[64,8,32]{2,1,0:T(8,128)S(1)} %broadcast_in_dim.72, f32[64,8,32]{2,1,0:T(8,128)S(1)} %broadcast_in_dim.71, f32[64,8,64]{2,1,0:T(8,128)S(1)} %bitcast.13), kind=kLoop, calls=%fused_computation | loop fusion | flops 131072 | bytes 524288 | tf_op jit(solution)/shard_map/concatenate | solution.py:331
  23.6 0.2 broadcast_in_dim.65
  23.8 0.1 broadcast_in_dim.66
  23.9 0.1 broadcast_in_dim.59
  24.0 0.1 broadcast_in_dim.60
  24.1 0.7 broadcast_select_fusion.q_ref
  24.8 15.8 %shard_map.137.packed = f32[64,8,128]{2,1,0:T(8,128)} custom-call(bf16[64,8,128]{2,1,0:T(8,128)(2,1)} %broadcast_select_fusion.q_ref, bf16[64,128,1024]{2,1,0:T(8,128)(2,1)} %bitcast.10, bf16[64,128,1024]{2,1,0:T(8,128)(2,1)} %bitcast.11, f32[64,8,1024]{2,1,0:T(8,128)} %d_ref.1), custom_call_target="tpu_custom_call" | custom-call | tf_op jit(solution)/shard_map/pallas_call | solution.py:347
  40.6 47.9 %shard_map.138 = bf16[64,512]{1,0:T(8,128)(2,1)} custom-call(f32[64,8,128]{2,1,0:T(8,128)} %shard_map.137.packed, f32[64,8,128]{2,1,0:T(8,128)} %pad_maximum_fusion.own, bf16[64,512]{1,0:T(8,128)(2,1)} %tok.3, f32[1,512]{1,0:T(1,128)} %bitcast.17, bf16[512,512]{1,0:T(8,128)(2,1)} %wo_hbm.1, bf16[512,4096]{1,0:T(8,128)(2,1)} %wu_hbm.1, bf16[4096,512]{1,0:T(8,128)(2,1)} %wd_hbm.1), custom_call_target="tpu_custom_call" | custom-call | tf_op jit(solution)/shard_map/pallas_call | solution.py:361
  88.5 1.5 %copy.21 = bf16[64,512]{1,0:T(8,128)(2,1)} copy(bf16[64,512]{1,0:T(8,128)(2,1)} %shard_map.138) | data formatting | bytes 131072
  (5 shorter events, 0.1 us)
